TPU v7x, 512 devices: a whole 4x4x16 slice. The times are simulated.
512 devices in a mesh: row: 64 (over z, y), col: 8 (over x, core).
Axes of the slice: x: 4, y: 4, z: 16, core: 2. Of those that a mesh axis runs over, the one named last changes fastest.
Arguments:
- tokens: bfloat16 [8, 12288, 2048], P('col', 'row'), may hold values from -6 to 6
- proj_in: bfloat16 [2048, 512], P('col'), may hold values from -0.125 to 0.125
- proj_out: bfloat16 [512, 2048], P(None, 'row'), may hold values from -0.25 to 0.25
Outputs:
- output: bfloat16 [8, 12288, 2048], P('col', 'row')
All inputs are finite; a program needn't handle non-finite values.
Results may differ from a plain program's by a relative error of at most 0.0083.
Values may be sent and summed in bfloat16 or wider, within the bound.
A program may use at most 64 MiB of HBM per device.

v0:
```python
import math
import jax
import jax.numpy as jnp
from jax import lax
from jax.sharding import Mesh
from jax.sharding import PartitionSpec as P

GRP = 128
ROW = ("row_0", "row_1")
highest = lax.Precision.HIGHEST
span_inner = 128


def copy_for_each(array, axis):
    copies = jnp.broadcast_to(array, (lax.axis_size(axis), *array.shape))
    return lax.all_to_all(copies, axis, split_axis=0, concat_axis=0, tiled=True)


def joined_along(tiles, dim):
    lengths = list(tiles.shape[1:])
    lengths[dim] *= tiles.shape[0]
    return jnp.moveaxis(tiles, 0, dim).reshape(lengths)


def gathered_copies(array, axis, dim):
    tiles = copy_for_each(array, axis)
    return joined_along(tiles, dim)


def in_blocks(array, dim, count):
    before, after = (array.shape[:dim], array.shape[dim + 1 :])
    return jnp.moveaxis(array.reshape(*before, count, -1, *after), dim, 0)


def turned_blocks(tiles, axes, sequence):
    inside = tiles.shape[1:]
    result = tiles.reshape(*(lax.axis_size(a) for a in axes), *inside)
    for k in sequence:
        result = lax.all_to_all(result, axes[k], k, k, tiled=True)
    return result.reshape(-1, *inside)


def exchange_by_axis(array, axes, sequence, split_dim, concat_dim):
    tiles = in_blocks(array, split_dim, lax.axis_size(axes))
    return joined_along(turned_blocks(tiles, axes, sequence), concat_dim)


def circle(height, breadth, period):
    product = lax.iota(jnp.int32, height)[:, None] * lax.iota(jnp.int32, breadth)[None, :] % period
    angle = product.astype(jnp.float32) * (2.0 * math.pi / period)
    return (jnp.cos(angle), jnp.sin(angle))


def mirror(values):
    return jnp.concatenate([values[:, :1], jnp.flip(values[:, 1:], 1)], 1)


def positions(piece):
    real_in = piece[0, 0]
    imag_in = piece[1, 0]
    count, length = real_in.shape
    outer = length // span_inner
    real_in = real_in.reshape(count, outer, span_inner)
    imag_in = imag_in.reshape(count, outer, span_inner)
    cos_one, sin_one = circle(outer, outer, outer)
    first_re = jnp.einsum("ab,kbq->kaq", cos_one, real_in, precision=highest) - jnp.einsum(
        "ab,kbq->kaq", sin_one, imag_in, precision=highest
    )
    first_im = jnp.einsum("ab,kbq->kaq", sin_one, real_in, precision=highest) + jnp.einsum(
        "ab,kbq->kaq", cos_one, imag_in, precision=highest
    )
    twist_c, twist_s = circle(outer, span_inner, length)
    turned_re = first_re * twist_c - first_im * twist_s
    turned_im = first_re * twist_s + first_im * twist_c
    cos_two, sin_two = circle(span_inner, span_inner, span_inner)
    factor = 1.0 / math.sqrt(GRP * length)
    real_out = jnp.einsum("kaq,qb->kba", turned_re, cos_two, precision=highest) - jnp.einsum(
        "kaq,qb->kba", turned_im, sin_two, precision=highest
    )
    real_out = real_out.reshape(count, length) * factor
    imag_out = jnp.einsum("kaq,qb->kba", turned_re, sin_two, precision=highest) + jnp.einsum(
        "kaq,qb->kba", turned_im, cos_two, precision=highest
    )
    imag_out = imag_out.reshape(count, length) * factor
    return jnp.stack([real_out, imag_out], 1)


def shards(tokens, proj_in, proj_out):
    seq_rows = tokens[0]
    local_len = seq_rows.shape[0]
    features = proj_in.shape[1]
    groups = features // GRP
    mapped = jnp.dot(
        seq_rows, gathered_copies(proj_in, "col", 0), preferred_element_type=jnp.float32
    ).astype(jnp.bfloat16)
    values = mapped.astype(jnp.float32).reshape(local_len, groups, GRP)
    cos_c, sin_c = circle(GRP, GRP, GRP)
    half = GRP // 2
    real_table = cos_c[:, :half]
    imag_table = jnp.concatenate([cos_c[:, half : half + 1], sin_c[:, 1:half]], 1)
    real_part = jnp.einsum("pgc,cs->gsp", values, real_table, precision=highest)
    imag_part = jnp.einsum("pgc,cs->gsp", values, imag_table, precision=highest)
    ways = lax.axis_size(ROW)
    slots = groups * real_table.shape[1]
    per_dev = slots // ways
    stacked = jnp.stack(
        [real_part.reshape(ways, per_dev, local_len), imag_part.reshape(ways, per_dev, local_len)],
        0,
    )
    spectra = positions(
        lax.all_to_all(
            stacked.astype(jnp.bfloat16), ROW, split_axis=1, concat_axis=3, tiled=True
        ).astype(stacked.dtype)
    )
    slot_ids = lax.axis_index(ROW) * per_dev + lax.iota(jnp.int32, per_dev)
    special = (slot_ids % half == 0)[:, None]
    real_g = spectra[:, 0]
    imag_g = spectra[:, 1]
    lower = jnp.where(special, 0.5 * (real_g + mirror(real_g)), real_g)
    upper = jnp.where(special, 0.5 * (imag_g + mirror(imag_g)), mirror(real_g))
    outgoing = jnp.stack([lower, upper], 1).astype(jnp.bfloat16)
    back = exchange_by_axis(outgoing, ROW, (0, 1), 2, 0)
    paired = back.reshape(groups, half, 2, local_len)
    low_half = paired[:, :, 0]
    high_half = paired[:, :, 1]
    mixed = jnp.concatenate([low_half, high_half[:, :1], jnp.flip(high_half[:, 1:], 1)], 1).reshape(
        features, local_len
    )
    result = lax.dot_general(
        mixed,
        lax.all_gather(proj_out, ROW, axis=1, tiled=True),
        (((0,), (0,)), ((), ())),
        preferred_element_type=jnp.float32,
    )
    return result.astype(jnp.bfloat16)[None]


def solution(mesh):
    split = Mesh(mesh.devices.reshape(16, 4, mesh.shape["col"]), ("row_0", "row_1", "col"))
    return jax.shard_map(
        shards,
        mesh=split,
        in_specs=(P("col", ROW, None), P("col", None), P(None, ROW)),
        out_specs=P("col", ROW, None),
        check_vma=False,
    )
```

profile of v0, /device:TPU:2, one launch (start us, length us, event | category | flops | bytes accessed | tf_op | source)
XLA Modules:
  0.0 218.3 jit_solution(16846580736775457972)
XLA Ops:
  6.5 2.5 %broadcast_in_dim.13 = bf16[8,256,512]{2,1,0:T(8,128)(2,1)} broadcast(bf16[256,512]{1,0:T(8,128)(2,1)} %param.4), dimensions={1,2} | broadcast | bytes 2359296 | tf_op jit(solution)/shard_map/broadcast_in_dim | solution.py:15
  9.1 9.4 %all-to-all-start = ((bf16[8,256,512]{2,1,0:T(8,128)(2,1)}), bf16[8,256,512]{2,1,0:T(8,128)(2,1)S(1)}, u32[]{:S(2)}, u32[]{:S(2)}) async-start(bf16[8,256,512]{2,1,0:T(8,128)(2,1)} %broadcast_in_dim.13), calls=%async_computation | async-start | bytes 4194304 | tf_op jit(solution)/shard_map/all_to_all | solution.py:16
  19.0 25.2 %all-to-all-done = bf16[8,256,512]{2,1,0:T(8,128)(2,1)S(1)} async-done(((bf16[8,256,512]{2,1,0:T(8,128)(2,1)}), bf16[8,256,512]{2,1,0:T(8,128)(2,1)S(1)}, u32[]{:S(2)}, u32[]{:S(2)}) %all-to-all-start) | async-done | bytes 2097184 | tf_op jit(solution)/shard_map/all_to_all | solution.py:16
  44.2 0.6 fusion.1
  44.8 0.5 fusion.8
  45.3 0.5 fusion.9
  45.9 0.9 pad_maximum_fusion
  46.8 14.1 %all-to-all-start.1 = ((bf16[2,64,4,192]{3,2,0,1:T(4,128)(2,1)}), bf16[2,64,4,192]{3,2,0,1:T(4,128)(2,1)S(1)}, u32[]{:S(2)}, u32[]{:S(2)}) async-start(bf16[2,64,4,192]{3,2,0,1:T(4,128)(2,1)} %pad_maximum_fusion), calls=%async_computation.1 | async-start | bytes 524288 | tf_op jit(solution)/shard_map/all_to_all | solution.py:111
  61.0 0.7 all-gather.2.cloned.1.call-update
  61.9 21.3 %all-to-all-done.1 = bf16[2,64,4,192]{3,2,0,1:T(4,128)(2,1)S(1)} async-done(((bf16[2,64,4,192]{3,2,0,1:T(4,128)(2,1)}), bf16[2,64,4,192]{3,2,0,1:T(4,128)(2,1)S(1)}, u32[]{:S(2)}, u32[]{:S(2)}) %all-to-all-start.1) | async-done | bytes 196640 | tf_op jit(solution)/shard_map/all_to_all | solution.py:111
  83.6 0.4 fusion.35
  84.0 0.4 fusion.31
  84.6 0.4 fusion.6
  85.0 0.4 fusion.7
  85.4 0.6 fusion.22
  86.0 0.6 fusion.5
  87.3 0.6 fusion.18
  87.8 0.6 fusion.3
  88.9 8.4 %reverse = f32[4,12288]{1,0:T(4,128)S(1)} reverse(f32[4,12288]{1,0:T(4,128)S(1)} %bitcast.99), dimensions={1} | reverse | bytes 393216
  97.6 8.4 %reverse.1 = f32[4,12288]{1,0:T(4,128)S(1)} reverse(f32[4,12288]{1,0:T(4,128)S(1)} %bitcast.100), dimensions={1} | reverse | bytes 393216
  107.3 20.6 %all_to_all.30 = bf16[16,4,4,2,192]{4,3,2,1,0:T(2,128)(2,1)S(1)} all-to-all(bf16[16,4,4,2,192]{4,3,2,1,0:T(2,128)(2,1)S(1)} %bitcast.98), channel_id=1, replica_groups=mesh['row_0'=16,'row_1'=4,'col'=8] {'row_0'}, dimensions={0} | all-to-all | bytes 393216 | tf_op jit(solution)/shard_map/all_to_all | solution.py:39
  128.2 9.7 %all_to_all.31 = bf16[16,4,4,2,192]{4,3,2,0,1:T(2,128)(2,1)S(1)} all-to-all(bf16[16,4,4,2,192]{4,3,2,0,1:T(2,128)(2,1)S(1)} %copy.77), channel_id=1, replica_groups=mesh['row_0'=16,'row_1'=4,'col'=8] {'row_1'}, dimensions={1} | all-to-all | bytes 393216 | tf_op jit(solution)/shard_map/all_to_all | solution.py:39
  138.8 69.3 %all-gather.2.cloned.1.call-done = bf16[512,2048]{0,1:T(8,128)(2,1)} async-done(((bf16[512,32]{0,1:T(8,128)(2,1)}), bf16[512,2048]{0,1:T(8,128)(2,1)}) %all-gather.2.cloned.1.call-update) | async-done | bytes 2097168 | tf_op jit(solution)/shard_map/all_gather | solution.py:131
  208.1 3.3 %fusion = bf16[1,192,2048]{2,1,0:T(8,128)(2,1)} fusion(bf16[512,192]{1,0:T(8,128)(2,1)S(1)} %bitcast.96, bf16[512,2048]{0,1:T(8,128)(2,1)} %all-gather.2.cloned.1.call-done), kind=kOutput, calls=%fused_computation.1 | convolution fusion | flops 403046400 | bytes 3080192 | tf_op jit(solution)/shard_map/dot_general | solution.py:129
  (45 shorter events, 5.3 us)
Async XLA Ops:
  6.5 37.7 %copy-start = (bf16[1,192,2048]{2,1,0:T(8,128)(2,1)S(1)}, bf16[1,192,2048]{2,1,0:T(8,128)(2,1)}, u32[]{:S(2)}) copy-start(bf16[1,192,2048]{2,1,0:T(8,128)(2,1)} %param.3) | copy-start | bytes 2359300
  9.1 35.1 %all-to-all-start = ((bf16[8,256,512]{2,1,0:T(8,128)(2,1)}), bf16[8,256,512]{2,1,0:T(8,128)(2,1)S(1)}, u32[]{:S(2)}, u32[]{:S(2)}) async-start(bf16[8,256,512]{2,1,0:T(8,128)(2,1)} %broadcast_in_dim.13), calls=%async_computation | async-start | bytes 4194304 | tf_op jit(solution)/shard_map/all_to_all | solution.py:16
  46.8 36.5 %all-to-all-start.1 = ((bf16[2,64,4,192]{3,2,0,1:T(4,128)(2,1)}), bf16[2,64,4,192]{3,2,0,1:T(4,128)(2,1)S(1)}, u32[]{:S(2)}, u32[]{:S(2)}) async-start(bf16[2,64,4,192]{3,2,0,1:T(4,128)(2,1)} %pad_maximum_fusion), calls=%async_computation.1 | async-start | bytes 524288 | tf_op jit(solution)/shard_map/all_to_all | solution.py:111
  60.9 147.2 %all-gather.2.cloned.1.call-start = ((), (), s32[]{:S(2)}) async-start(), calls=%async_computation.4 | async-start | bytes 2129920 | tf_op jit(solution)/shard_map/all_gather | solution.py:131
Sparse Core Ops, SparseCore 0:
  64.7 143.3 all-gather.1
where the time goes:
time: 219 us; the launch traced here: 218 us
  waiting for transfers between devices  116 us (53%)
  blocking collectives  30.3 us (14%)
  starting transfers between devices  23.6 us (11%)
  local copies, waits for them, and re-layouts  23.1 us (11%)
  between operations  13.7 us (6%)
  matrix products  8.83 us (4%)
  other arithmetic  2.26 us (1%)
    all_gather x1, waiting for transfers between devices, shards(): lax.all_gather(proj_out, ROW, axis=1, tiled=True)  69.3 us
    all_to_all x2, blocking collectives, turned_blocks(): result = lax.all_to_all(result, axes[k], k, k, tiled=True)  30.3 us
    all_to_all x1, waiting for transfers between devices, copy_for_each(): return lax.all_to_all(copies, axis, split_axis=0, concat_axis=0, tiled=True)  25.2 us
    all_to_all x1, waiting for transfers between devices, shards(): lax.all_to_all(stacked.astype(jnp.bfloat16), ROW, split_axis=1, concat_ax...  21.3 us
    unnamed x6, local copies, waits for them, and re-layouts  16.8 us
    all_to_all x1, starting transfers between devices, shards(): lax.all_to_all(stacked.astype(jnp.bfloat16), ROW, split_axis=1, concat_ax...  14.1 us
    all_to_all x1, starting transfers between devices, copy_for_each(): return lax.all_to_all(copies, axis, split_axis=0, concat_axis=0, tiled=True)  9.39 us
  transfers between devices with their start and end apart: 3, of which 3 were waited for; matrix products, arithmetic and copies ran while one was open for 12% of the time, Pallas kernels for 0%

commit v1 on v0

--- a/solution.py
+++ b/solution.py
@@ -128,7 +128,9 @@
     )
     result = lax.dot_general(
         mixed,
-        lax.all_gather(proj_out, ROW, axis=1, tiled=True),
+        jnp.concatenate(
+            lax.all_to_all(jnp.stack([proj_out] * lax.axis_size(ROW)), ROW, 0, 0), axis=1
+        ),
         (((0,), (0,)), ((), ())),
         preferred_element_type=jnp.float32,
     )

time: 219 us -> 240 us (1.096)
  the two profiles are of different devices: /device:TPU:2 before, /device:TPU:8 now
where the time goes in v1:
time: 240 us
  waiting for transfers between devices  144 us (60%)
  starting transfers between devices  31 us (13%)
  blocking collectives  30 us (12%)
  local copies, waits for them, and re-layouts  24.7 us (10%)
  matrix products  7.24 us (3%)
    all_to_all x1, waiting for transfers between devices, shards(): lax.all_to_all(jnp.stack([proj_out] * lax.axis_size(ROW)), ROW, 0, 0)  96.6 us
    all_to_all x2, blocking collectives, turned_blocks(): result = lax.all_to_all(result, axes[k], k, k, tiled=True)  30 us
    all_to_all x1, waiting for transfers between devices, copy_for_each(): return lax.all_to_all(copies, axis, split_axis=0, concat_axis=0, tiled=True)  26.6 us
    all_to_all x1, waiting for transfers between devices, shards(): lax.all_to_all(stacked.astype(jnp.bfloat16), ROW, split_axis=1, concat_ax...  21 us
    all_to_all x1, starting transfers between devices, shards(): lax.all_to_all(stacked.astype(jnp.bfloat16), ROW, split_axis=1, concat_ax...  18.7 us
    unnamed x8, local copies, waits for them, and re-layouts  16.8 us
    all_to_all x1, starting transfers between devices, shards(): lax.all_to_all(jnp.stack([proj_out] * lax.axis_size(ROW)), ROW, 0, 0)  7.93 us
  transfers between devices with their start and end apart: 3, of which 3 were waited for; matrix products, arithmetic and copies ran while one was open for 1% of the time, Pallas kernels for 0%

profile of v1, /device:TPU:8, one launch (start us, length us, event | category | flops | bytes accessed | tf_op | source)
XLA Modules:
  0.0 239.7 jit_solution(14200561163914746593)
XLA Ops:
  0.0 2.5 %broadcast_in_dim.13 = bf16[8,256,512]{2,1,0:T(8,128)(2,1)} broadcast(bf16[256,512]{1,0:T(8,128)(2,1)} %param.4), dimensions={1,2} | broadcast | bytes 2359296 | tf_op jit(solution)/shard_map/broadcast_in_dim | solution.py:15
  2.5 4.3 %all-to-all-start = ((bf16[8,256,512]{2,1,0:T(8,128)(2,1)}), bf16[8,256,512]{2,1,0:T(8,128)(2,1)S(1)}, u32[]{:S(2)}, u32[]{:S(2)}) async-start(bf16[8,256,512]{2,1,0:T(8,128)(2,1)} %broadcast_in_dim.13), calls=%async_computation | async-start | bytes 4194304 | tf_op jit(solution)/shard_map/all_to_all | solution.py:16
  7.4 26.6 %all-to-all-done = bf16[8,256,512]{2,1,0:T(8,128)(2,1)S(1)} async-done(((bf16[8,256,512]{2,1,0:T(8,128)(2,1)}), bf16[8,256,512]{2,1,0:T(8,128)(2,1)S(1)}, u32[]{:S(2)}, u32[]{:S(2)}) %all-to-all-start) | async-done | bytes 2097184 | tf_op jit(solution)/shard_map/all_to_all | solution.py:16
  34.0 0.6 fusion.1
  34.6 0.5 fusion.8
  35.1 0.5 fusion.9
  35.7 0.9 pad_maximum_fusion
  36.6 18.7 %all-to-all-start.1 = ((bf16[2,64,4,192]{3,2,0,1:T(4,128)(2,1)}), bf16[2,64,4,192]{3,2,0,1:T(4,128)(2,1)S(1)}, u32[]{:S(2)}, u32[]{:S(2)}) async-start(bf16[2,64,4,192]{3,2,0,1:T(4,128)(2,1)} %pad_maximum_fusion), calls=%async_computation.1 | async-start | bytes 524288 | tf_op jit(solution)/shard_map/all_to_all | solution.py:111
  55.6 21.0 %all-to-all-done.1 = bf16[2,64,4,192]{3,2,0,1:T(4,128)(2,1)S(1)} async-done(((bf16[2,64,4,192]{3,2,0,1:T(4,128)(2,1)}), bf16[2,64,4,192]{3,2,0,1:T(4,128)(2,1)S(1)}, u32[]{:S(2)}, u32[]{:S(2)}) %all-to-all-start.1) | async-done | bytes 196640 | tf_op jit(solution)/shard_map/all_to_all | solution.py:111
  76.9 0.4 fusion.31
  77.9 0.4 fusion.7
  78.3 0.4 fusion.6
  78.8 0.6 fusion.18
  79.3 0.6 fusion.3
  80.6 0.6 fusion.22
  81.2 0.6 fusion.5
  82.4 8.4 %reverse.1 = f32[4,12288]{1,0:T(4,128)S(1)} reverse(f32[4,12288]{1,0:T(4,128)S(1)} %bitcast.103), dimensions={1} | reverse | bytes 393216
  91.3 8.4 %reverse = f32[4,12288]{1,0:T(4,128)S(1)} reverse(f32[4,12288]{1,0:T(4,128)S(1)} %bitcast.104), dimensions={1} | reverse | bytes 393216
  100.7 20.3 %all_to_all.35 = bf16[16,4,4,2,192]{4,3,2,1,0:T(2,128)(2,1)S(1)} all-to-all(bf16[16,4,4,2,192]{4,3,2,1,0:T(2,128)(2,1)S(1)} %bitcast.102), channel_id=1, replica_groups=mesh['row_0'=16,'row_1'=4,'col'=8] {'row_0'}, dimensions={0} | all-to-all | bytes 393216 | tf_op jit(solution)/shard_map/all_to_all | solution.py:39
  121.2 9.7 %all_to_all.36 = bf16[16,4,4,2,192]{4,3,2,0,1:T(2,128)(2,1)S(1)} all-to-all(bf16[16,4,4,2,192]{4,3,2,0,1:T(2,128)(2,1)S(1)} %copy.78), channel_id=1, replica_groups=mesh['row_0'=16,'row_1'=4,'col'=8] {'row_1'}, dimensions={1} | all-to-all | bytes 393216 | tf_op jit(solution)/shard_map/all_to_all | solution.py:39
  130.9 1.6 stack.9
  132.5 7.9 %all-to-all-start.4 = ((bf16[64,512,32]{1,2,0:T(8,128)(2,1)}), bf16[64,512,32]{1,2,0:T(8,128)(2,1)S(1)}, u32[]{:S(2)}, u32[]{:S(2)}) async-start(bf16[64,512,32]{1,2,0:T(8,128)(2,1)} %stack.9), calls=%async_computation.4 | async-start | bytes 4194304 | tf_op jit(solution)/shard_map/all_to_all | solution.py:132
  141.4 96.6 %all-to-all-done.4 = bf16[64,512,32]{1,2,0:T(8,128)(2,1)S(1)} async-done(((bf16[64,512,32]{1,2,0:T(8,128)(2,1)}), bf16[64,512,32]{1,2,0:T(8,128)(2,1)S(1)}, u32[]{:S(2)}, u32[]{:S(2)}) %all-to-all-start.4) | async-done | bytes 2097184 | tf_op jit(solution)/shard_map/all_to_all | solution.py:132
  238.0 1.7 fusion
  (47 shorter events, 5.6 us)
Async XLA Ops:
  0.0 34.0 %copy-start = (bf16[1,192,2048]{2,1,0:T(8,128)(2,1)S(1)}, bf16[1,192,2048]{2,1,0:T(8,128)(2,1)}, u32[]{:S(2)}) copy-start(bf16[1,192,2048]{2,1,0:T(8,128)(2,1)} %param.3) | copy-start | bytes 2359300
  2.5 31.5 %all-to-all-start = ((bf16[8,256,512]{2,1,0:T(8,128)(2,1)}), bf16[8,256,512]{2,1,0:T(8,128)(2,1)S(1)}, u32[]{:S(2)}, u32[]{:S(2)}) async-start(bf16[8,256,512]{2,1,0:T(8,128)(2,1)} %broadcast_in_dim.13), calls=%async_computation | async-start | bytes 4194304 | tf_op jit(solution)/shard_map/all_to_all | solution.py:16
  36.6 40.0 %all-to-all-start.1 = ((bf16[2,64,4,192]{3,2,0,1:T(4,128)(2,1)}), bf16[2,64,4,192]{3,2,0,1:T(4,128)(2,1)S(1)}, u32[]{:S(2)}, u32[]{:S(2)}) async-start(bf16[2,64,4,192]{3,2,0,1:T(4,128)(2,1)} %pad_maximum_fusion), calls=%async_computation.1 | async-start | bytes 524288 | tf_op jit(solution)/shard_map/all_to_all | solution.py:111
  100.1 30.7 %copy-start.1 = (bf16[512,32]{0,1:T(8,128)(2,1)S(1)}, bf16[512,32]{0,1:T(8,128)(2,1)}, u32[]{:S(2)}) copy-start(bf16[512,32]{0,1:T(8,128)(2,1)} %param.5) | copy-start | bytes 98308
  132.5 105.5 %all-to-all-start.4 = ((bf16[64,512,32]{1,2,0:T(8,128)(2,1)}), bf16[64,512,32]{1,2,0:T(8,128)(2,1)S(1)}, u32[]{:S(2)}, u32[]{:S(2)}) async-start(bf16[64,512,32]{1,2,0:T(8,128)(2,1)} %stack.9), calls=%async_computation.4 | async-start | bytes 4194304 | tf_op jit(solution)/shard_map/all_to_all | solution.py:132
